TPU v7x, 32 devices: a whole 2x2x4 slice. The times are simulated.
32 devices in a mesh: tp: 8 (over z, y), dp: 4 (over x, core).
Axes of the slice: x: 2, y: 2, z: 4, core: 2. Of those that a mesh axis runs over, the one named last changes fastest.
Arguments:
- tokens: bfloat16 [128, 4096], P('tp', 'dp'), may hold values from -10 to 10
- norm_gain: float32 [2, 4096], P(None, 'dp'), may hold values from 0.1 to 1.9
- input_weight: bfloat16 [2, 4096, 1024], P(None, 'dp', 'tp'), may hold values from -0.09375 to 0.09375
- decay_rate: float32 [2, 64, 64], P(None, 'tp'), may hold values from 0.01 to 1
- frequency: float32 [2, 64, 64], P(None, 'tp'), may hold values from 0.5 to 3
- step_size: float32 [2, 64], P(None, 'tp'), may hold values from 0.1 to 1
- state_in: float32 [2, 64, 16, 128], P(None, 'tp'), may hold values from -1.5 to 1.5
- readout: float32 [2, 64, 16, 128], P(None, 'tp'), may hold values from -0.5 to 0.5
- skip_gain: float32 [2, 1024], P(None, 'tp'), may hold values from -3 to 3
- value_weight: bfloat16 [2, 1024, 4096], P(None, 'tp', 'dp'), may hold values from -0.1875 to 0.1875
- gate_weight: bfloat16 [2, 1024, 4096], P(None, 'tp', 'dp'), may hold values from -0.1875 to 0.1875
- states: float32 [2, 128, 64, 128], P(None, 'dp', 'tp'), may hold values from -3 to 3
Outputs:
- tokens_out: bfloat16 [128, 4096], P('tp', 'dp')
- states_out: float32 [2, 128, 64, 128], P(None, 'dp', 'tp')
All inputs are finite; a program needn't handle non-finite values.
Results may differ from a plain program's by a relative error of at most 0.007.
Values may be sent and summed in bfloat16 or wider, within the bound.
No kernel may reach another device: no remote copies, remote signals or barrier semaphores. Data moves between devices by JAX's collectives and lax.ppermute only.
A program may use at most 64 MiB of HBM per device.

v0:
```python
import jax
import jax.numpy as jnp
from jax import lax
from jax.sharding import PartitionSpec as P

D = 4096
LAYERS = 2
epsilon = 1e-06


def transition(rate, frequency, step):
    magnitude = jnp.exp(-rate * step[:, None])
    angle = frequency * step[:, None]
    keep_real = magnitude * jnp.cos(angle)
    keep_imag = magnitude * jnp.sin(angle)
    minus_one = keep_real - 1.0
    denominator = rate * rate + frequency * frequency
    lift_real = (-minus_one * rate + keep_imag * frequency) / denominator
    lift_imag = (-keep_imag * rate - minus_one * frequency) / denominator
    return (keep_real, keep_imag, lift_real, lift_imag)


def update(drive, state, rate, frequency, step, state_in, readout, skip):
    groups = rate.shape[0]
    half = state.shape[-1] // 2
    grouped = drive.reshape(drive.shape[0], groups, -1)
    pushed = jnp.einsum("sgc,gcq->sgq", grouped, state_in, precision=lax.Precision.HIGHEST)
    keep_real, keep_imag, lift_real, lift_imag = transition(rate, frequency, step)
    push_real, push_imag = (pushed[..., :half], pushed[..., half:])
    old_real, old_imag = (state[..., :half], state[..., half:])
    new_real = (
        keep_real * old_real - keep_imag * old_imag + lift_real * push_real - lift_imag * push_imag
    )
    new_imag = (
        keep_real * old_imag + keep_imag * old_real + lift_real * push_imag + lift_imag * push_real
    )
    new_state = jnp.concatenate([new_real, new_imag], axis=-1)
    summed = jnp.einsum("sgq,gcq->sgc", new_state, readout, precision=lax.Precision.HIGHEST)
    value = summed.reshape(drive.shape) + skip[None, :] * drive
    return (new_state, jax.nn.gelu(value).astype(jnp.bfloat16))


def body(
    tokens,
    norm_gain,
    input_weight,
    decay_rate,
    frequency,
    step_size,
    state_in,
    readout,
    skip_gain,
    value_weight,
    gate_weight,
    states,
):
    current = tokens
    own_rows = states.shape[1]
    offset = lax.axis_index("dp") * own_rows
    width_dev = tokens.shape[1]
    updated = []
    for depth_index in range(LAYERS):
        whole = lax.all_gather(current, "tp", axis=0, tiled=True)
        widened = whole.astype(jnp.float32)
        squares = jnp.sum(widened * widened, axis=1)
        gained = (widened * norm_gain[depth_index][None, :]).astype(jnp.bfloat16)
        weight_in = input_weight[depth_index]
        totals = lax.psum(squares, "dp")
        own_squares = lax.dynamic_slice_in_dim(totals, offset, own_rows)
        summed = lax.psum_scatter(
            jnp.dot(gained, weight_in, preferred_element_type=jnp.float32),
            "dp",
            scatter_dimension=0,
            tiled=True,
        )
        drive = summed * lax.rsqrt(own_squares / D + epsilon)[:, None]
        new_state, readout_value = update(
            drive,
            states[depth_index],
            decay_rate[depth_index],
            frequency[depth_index],
            step_size[depth_index],
            state_in[depth_index],
            readout[depth_index],
            skip_gain[depth_index],
        )
        updated.append(new_state)
        ready = lax.all_gather(readout_value, "dp", axis=0, tiled=True)
        value_rows = value_weight[depth_index]
        gate_rows = gate_weight[depth_index]
        both = lax.psum_scatter(
            jnp.concatenate(
                [
                    jnp.dot(ready, value_rows, preferred_element_type=jnp.float32),
                    jnp.dot(ready, gate_rows, preferred_element_type=jnp.float32),
                ],
                axis=1,
            ),
            "tp",
            scatter_dimension=0,
            tiled=True,
        )
        value, gate = (both[:, :width_dev], both[:, width_dev:])
        current = (current.astype(jnp.float32) + value * jax.nn.sigmoid(gate)).astype(jnp.bfloat16)
    return (current, jnp.stack(updated))


def solution(mesh):
    in_specs = (
        P("tp", "dp"),
        P(None, "dp"),
        P(None, "dp", "tp"),
        P(None, "tp", None),
        P(None, "tp", None),
        P(None, "tp"),
        P(None, "tp", None, None),
        P(None, "tp", None, None),
        P(None, "tp"),
        P(None, "tp", "dp"),
        P(None, "tp", "dp"),
        P(None, "dp", "tp", None),
    )
    out_specs = (P("tp", "dp"), P(None, "dp", "tp", None))
    return jax.shard_map(body, mesh=mesh, in_specs=in_specs, out_specs=out_specs, check_vma=False)
```

profile of v0, /device:TPU:0, one launch (start us, length us, event | category | flops | bytes accessed | tf_op | source)
XLA Modules:
  0.0 270.4 jit_solution(15485128415687994219)
XLA Ops:
  7.2 0.8 fusion.73
  8.0 32.8 %all_gather.12 = bf16[128,1024]{1,0:T(8,128)(2,1)S(1)} all-gather(bf16[16,1024]{1,0:T(8,128)(2,1)} %param.12), channel_id=1, replica_groups=mesh['tp'=8,'dp'=4] {'tp'}, dimensions={0}, use_global_device_ids=true | all-gather | bytes 294912 | tf_op jit(solution)/shard_map/all_gather | solution.py:63
  40.8 1.8 fusion.6
  42.7 0.6 copy-done.10
  43.4 0.6 copy-done.8
  44.3 5.8 %psum.14 = f32[128]{0:T(128)S(1)} all-reduce(f32[128]{0:T(128)S(1)} %fusion.1), channel_id=1, replica_groups=mesh['tp'=8,'dp'=4] {'dp'}, use_global_device_ids=true, to_apply=%region_2.0 | all-reduce | flops 128 | bytes 1024 | tf_op jit(solution)/shard_map/psum | solution.py:68
  50.2 13.1 %reduce-scatter.5.cloned.1.call-done = f32[32,128]{1,0:T(8,128)} async-done(((f32[128,128]{1,0:T(8,128)}), f32[32,128]{1,0:T(8,128)}) %reduce-scatter.5.cloned.1.call-update) | async-done | bytes 16400 | tf_op jit(solution)/shard_map/reduce_scatter | solution.py:70
  63.4 0.8 broadcast_multiply_fusion.1
  64.2 0.4 convolution_bitcast_fusion.1
  64.8 0.7 copy-done.5
  65.6 0.4 fusion.39
  66.0 0.2 copy-done.6
  66.4 5.2 %all_gather.13 = bf16[128,128]{1,0:T(8,128)(2,1)S(1)} all-gather(bf16[32,128]{1,0:T(8,128)(2,1)S(1)} %fusion.57), channel_id=1, replica_groups=mesh['tp'=8,'dp'=4] {'dp'}, dimensions={0}, use_global_device_ids=true | all-gather | bytes 40960 | tf_op jit(solution)/shard_map/all_gather | solution.py:88
  71.6 0.2 fusion.13
  71.8 0.2 fusion.15
  72.0 1.0 pad_maximum_fusion
  73.1 64.3 %reduce-scatter.7.cloned.1.call-done = f32[16,2048]{1,0:T(8,128)} async-done(((f32[128,2048]{1,0:T(8,128)}), f32[16,2048]{1,0:T(8,128)}) %reduce-scatter.7.cloned.1.call-update) | async-done | bytes 131088 | tf_op jit(solution)/shard_map/reduce_scatter | solution.py:91
  137.4 0.9 fusion.46
  138.3 30.8 %all_gather.14 = bf16[128,1024]{1,0:T(8,128)(2,1)S(1)} all-gather(bf16[16,1024]{1,0:T(8,128)(2,1)S(1)} %fusion.46), channel_id=1, replica_groups=mesh['tp'=8,'dp'=4] {'tp'}, dimensions={0}, use_global_device_ids=true | all-gather | bytes 294912 | tf_op jit(solution)/shard_map/all_gather | solution.py:63
  169.2 0.9 fusion.4
  170.3 5.7 %psum.15 = f32[128]{0:T(128)S(1)} all-reduce(f32[128]{0:T(128)S(1)} %fusion.3), channel_id=1, replica_groups=mesh['tp'=8,'dp'=4] {'dp'}, use_global_device_ids=true, to_apply=%region_6.0 | all-reduce | flops 128 | bytes 1024 | tf_op jit(solution)/shard_map/psum | solution.py:68
  176.0 12.6 %reduce-scatter.9.cloned.1.call-done = f32[32,128]{1,0:T(8,128)} async-done(((f32[128,128]{1,0:T(8,128)}), f32[32,128]{1,0:T(8,128)}) %reduce-scatter.9.cloned.1.call-update) | async-done | bytes 16400 | tf_op jit(solution)/shard_map/reduce_scatter | solution.py:70
  188.6 0.8 broadcast_multiply_fusion
  189.5 0.4 convolution_bitcast_fusion
  190.1 0.4 fusion.36
  190.6 0.7 copy-done.7
  191.3 5.2 %all_gather.15 = bf16[128,128]{1,0:T(8,128)(2,1)S(1)} all-gather(bf16[32,128]{1,0:T(8,128)(2,1)S(1)} %fusion.65), channel_id=1, replica_groups=mesh['tp'=8,'dp'=4] {'dp'}, dimensions={0}, use_global_device_ids=true | all-gather | bytes 40960 | tf_op jit(solution)/shard_map/all_gather | solution.py:88
  196.7 0.2 fusion.10
  196.9 1.0 pad_maximum_fusion.1
  198.2 0.9 copy.27
  199.1 63.2 %reduce-scatter.11.cloned.1.call-done = f32[16,2048]{1,0:T(8,128)} async-done(((f32[128,2048]{1,0:T(8,128)}), f32[16,2048]{1,0:T(8,128)}) %reduce-scatter.11.cloned.1.call-update) | async-done | bytes 131088 | tf_op jit(solution)/shard_map/reduce_scatter | solution.py:91
  262.4 1.5 fusion.47
  (50 shorter events, 2.1 us)
Async XLA Ops:
  7.2 56.2 %reduce-scatter.5.cloned.1.call-start = ((), (), s32[]{:S(2)}) async-start(), calls=%async_computation.4 | async-start | bytes 81920 | tf_op jit(solution)/shard_map/reduce_scatter | solution.py:70
  40.8 2.6 copy-start.2
  42.6 0.7 copy-start.10
  42.6 0.7 copy-start.11
  42.7 94.8 %reduce-scatter.7.cloned.1.call-start = ((), (), s32[]{:S(2)}) async-start(), calls=%async_computation.5 | async-start | bytes 1179648 | tf_op jit(solution)/shard_map/reduce_scatter | solution.py:91
  43.4 0.7 copy-start.8
  43.4 0.7 copy-start.9
  44.3 19.9 %copy-start.4 = (f32[2,8,16,128]{3,2,1,0:T(8,128)S(1)}, f32[2,8,16,128]{3,2,1,0:T(8,128)}, u32[]{:S(2)}) copy-start(f32[2,8,16,128]{3,2,1,0:T(8,128)} %param.18) | copy-start | bytes 393220
  64.7 0.9 copy-start.5
  64.7 6.9 %copy-start = (bf16[2,128,1024]{2,1,0:T(8,128)(2,1)S(1)}, bf16[2,128,1024]{2,1,0:T(8,128)(2,1)}, u32[]{:S(2)}) copy-start(bf16[2,128,1024]{2,1,0:T(8,128)(2,1)} %param.22) | copy-start | bytes 1572868
  65.6 0.7 copy-start.6
  66.0 5.8 %copy-start.1 = (bf16[2,128,1024]{2,1,0:T(8,128)(2,1)S(1)}, bf16[2,128,1024]{2,1,0:T(8,128)(2,1)}, u32[]{:S(2)}) copy-start(bf16[2,128,1024]{2,1,0:T(8,128)(2,1)} %param.21) | copy-start | bytes 1572868
  73.1 64.4 %copy-start.3 = (bf16[16,1024]{1,0:T(8,128)(2,1)S(1)}, bf16[16,1024]{1,0:T(8,128)(2,1)}, u32[]{:S(2)}) copy-start(bf16[16,1024]{1,0:T(8,128)(2,1)} %param.12) | copy-start | bytes 98308
  73.1 96.1 %copy-start.12 = (bf16[2,1024,128]{2,1,0:T(8,128)(2,1)S(1)}, bf16[2,1024,128]{2,1,0:T(8,128)(2,1)}, u32[]{:S(2)}) copy-start(bf16[2,1024,128]{2,1,0:T(8,128)(2,1)} %param.14) | copy-start | bytes 1572868
  73.1 115.5 %reduce-scatter.9.cloned.1.call-start = ((), (), s32[]{:S(2)}) async-start(), calls=%async_computation.6 | async-start | bytes 81920 | tf_op jit(solution)/shard_map/reduce_scatter | solution.py:70
  170.1 92.3 %reduce-scatter.11.cloned.1.call-start = ((), (), s32[]{:S(2)}) async-start(), calls=%async_computation.7 | async-start | bytes 1179648 | tf_op jit(solution)/shard_map/reduce_scatter | solution.py:91
  190.5 0.7 copy-start.7
Sparse Core Ops, SparseCore 0:
  42.8 20.5 reduce-scatter.4
  73.2 64.1 reduce-scatter.6
  170.2 18.3 reduce-scatter.8
  198.1 64.1 reduce-scatter.10
where the time goes:
time: 271 us; the launch traced here: 270 us
  waiting for transfers between devices  153 us (56%)
  blocking collectives  85.4 us (32%)
  between operations  14 us (5%)
  other arithmetic  7.3 us (3%)
  matrix products  5.18 us (2%)
  local copies, waits for them, and re-layouts  4.96 us (2%)
    reduce_scatter x2, waiting for transfers between devices, body(): lax.psum_scatter(jnp.concatenate([jnp.dot(ready, value_rows, preferred_el...  128 us
    all_gather x2, blocking collectives, body(): whole = lax.all_gather(current, 'tp', axis=0, tiled=True)  63.6 us
    reduce_scatter x2, waiting for transfers between devices, body(): lax.psum_scatter(jnp.dot(gained, weight_in, preferred_element_type=jnp.fl...  25.8 us
    psum x2, blocking collectives, body(): totals = lax.psum(squares, 'dp')  11.5 us
    all_gather x2, blocking collectives, body(): ready = lax.all_gather(readout_value, 'dp', axis=0, tiled=True)  10.4 us
  transfers between devices with their start and end apart: 4, of which 4 were waited for; matrix products, arithmetic and copies ran while one was open for 1% of the time, Pallas kernels for 0%

commit v1 on v0

--- a/solution.py
+++ b/solution.py
@@ -60,7 +60,14 @@
     width_dev = tokens.shape[1]
     updated = []
     for depth_index in range(LAYERS):
-        whole = lax.all_gather(current, "tp", axis=0, tiled=True)
+        ring = [current]
+        for hop in range(7):
+            ring.append(lax.ppermute(ring[-1], "tp", [(dev, (dev + 1) % 8) for dev in range(8)]))
+        whole = jnp.roll(
+            jnp.concatenate(ring[::-1], axis=0),
+            (lax.axis_index("tp") + 1) * ring[0].shape[0],
+            axis=0,
+        )
         widened = whole.astype(jnp.float32)
         squares = jnp.sum(widened * widened, axis=1)
         gained = (widened * norm_gain[depth_index][None, :]).astype(jnp.bfloat16)

time: 271 us -> 296 us (1.092)
  waiting for transfers between devices: 153 us -> 239 us
  blocking collectives: 85.4 us -> 21.7 us
  starting transfers between devices: 0.16 us -> 4.35 us
    ppermute x0 -> x14, waiting for transfers between devices: none -> 89.2 us  [body(): lax.ppermute(ring[-1], 'tp', [(dev, (dev + 1) % 8) for dev in range(8)])]
    all_gather x2 -> x0, blocking collectives: 63.6 us -> none  [body(): whole = lax.all_gather(current, 'tp', axis=0, tiled=True)]
    ppermute x0 -> x14, starting transfers between devices: none -> 4.19 us  [body(): lax.ppermute(ring[-1], 'tp', [(dev, (dev + 1) % 8) for dev in range(8)])]
    reduce_scatter x2, waiting for transfers between devices: 25.8 us -> 21.9 us  [body(): lax.psum_scatter(jnp.dot(gained, weight_in, preferred_element_type=jnp.fl...]
  transfers between devices with their start and end apart: 4 -> 18, of which waited for: 4 -> 18; matrix products, arithmetic and copies ran while one was open for 1% -> 1% of each run, Pallas kernels for 0% -> 0%
where the time goes in v1:
time: 296 us; the launch traced here: 295 us
  waiting for transfers between devices  239 us (81%)
  blocking collectives  21.7 us (7%)
  between operations  14.1 us (5%)
  other arithmetic  7.55 us (3%)
  local copies, waits for them, and re-layouts  4.72 us (2%)
  starting transfers between devices  4.35 us (1%)
  matrix products  4.32 us (1%)
    reduce_scatter x2, waiting for transfers between devices, body(): lax.psum_scatter(jnp.concatenate([jnp.dot(ready, value_rows, preferred_el...  128 us
    ppermute x14, waiting for transfers between devices, body(): lax.ppermute(ring[-1], 'tp', [(dev, (dev + 1) % 8) for dev in range(8)])  89.2 us
    reduce_scatter x2, waiting for transfers between devices, body(): lax.psum_scatter(jnp.dot(gained, weight_in, preferred_element_type=jnp.fl...  21.9 us
    psum x2, blocking collectives, body(): totals = lax.psum(squares, 'dp')  11.3 us
    all_gather x2, blocking collectives, body(): ready = lax.all_gather(readout_value, 'dp', axis=0, tiled=True)  10.4 us
  transfers between devices with their start and end apart: 18, of which 18 were waited for; matrix products, arithmetic and copies ran while one was open for 1% of the time, Pallas kernels for 0%

profile of v1, /device:TPU:0, one launch (start us, length us, event | category | flops | bytes accessed | tf_op | source)
XLA Modules:
  0.0 295.5 jit_solution(9293903349074095734)
XLA Ops:
  7.2 3.0 %collective-permute-start = (bf16[16,1024]{1,0:T(8,128)(2,1)}, bf16[16,1024]{1,0:T(8,128)(2,1)S(1)}, u32[]{:S(2)}, u32[]{:S(2)}) collective-permute-start(bf16[16,1024]{1,0:T(8,128)(2,1)} %param.14), channel_id=1, source_target_pairs={{0,4},{4,8},{8,12},{12,16},{16,20},{20,24},{24,28},{28,0},{1,5},{5... | collective-permute-start | bytes 98312 | tf_op jit(solution)/shard_map/ppermute | solution.py:65
  10.3 5.1 %collective-permute-done = bf16[16,1024]{1,0:T(8,128)(2,1)S(1)} collective-permute-done((bf16[16,1024]{1,0:T(8,128)(2,1)}, bf16[16,1024]{1,0:T(8,128)(2,1)S(1)}, u32[]{:S(2)}, u32[]{:S(2)}) %collective-permute-start) | collective-permute-done | bytes 32800 | tf_op jit(solution)/shard_map/ppermute | solution.py:65
  15.4 1.0 fusion.76
  16.4 5.6 %collective-permute-done.1 = bf16[16,1024]{1,0:T(8,128)(2,1)S(1)} collective-permute-done((bf16[16,1024]{1,0:T(8,128)(2,1)S(1)}, bf16[16,1024]{1,0:T(8,128)(2,1)S(1)}, u32[]{:S(2)}, u32[]{:S(2)}) %collective-permute-start.1) | collective-permute-done | bytes 32800 | tf_op jit(solution)/shard_map/ppermute | solution.py:65
  22.1 6.5 %collective-permute-done.2 = bf16[16,1024]{1,0:T(8,128)(2,1)S(1)} collective-permute-done((bf16[16,1024]{1,0:T(8,128)(2,1)S(1)}, bf16[16,1024]{1,0:T(8,128)(2,1)S(1)}, u32[]{:S(2)}, u32[]{:S(2)}) %collective-permute-start.2) | collective-permute-done | bytes 32800 | tf_op jit(solution)/shard_map/ppermute | solution.py:65
  28.6 6.6 %collective-permute-done.3 = bf16[16,1024]{1,0:T(8,128)(2,1)S(1)} collective-permute-done((bf16[16,1024]{1,0:T(8,128)(2,1)S(1)}, bf16[16,1024]{1,0:T(8,128)(2,1)S(1)}, u32[]{:S(2)}, u32[]{:S(2)}) %collective-permute-start.3) | collective-permute-done | bytes 32800 | tf_op jit(solution)/shard_map/ppermute | solution.py:65
  35.4 6.8 %collective-permute-done.4 = bf16[16,1024]{1,0:T(8,128)(2,1)S(1)} collective-permute-done((bf16[16,1024]{1,0:T(8,128)(2,1)S(1)}, bf16[16,1024]{1,0:T(8,128)(2,1)S(1)}, u32[]{:S(2)}, u32[]{:S(2)}) %collective-permute-start.4) | collective-permute-done | bytes 32800 | tf_op jit(solution)/shard_map/ppermute | solution.py:65
  42.2 6.6 %collective-permute-done.5 = bf16[16,1024]{1,0:T(8,128)(2,1)S(1)} collective-permute-done((bf16[16,1024]{1,0:T(8,128)(2,1)S(1)}, bf16[16,1024]{1,0:T(8,128)(2,1)S(1)}, u32[]{:S(2)}, u32[]{:S(2)}) %collective-permute-start.5) | collective-permute-done | bytes 32800 | tf_op jit(solution)/shard_map/ppermute | solution.py:65
  48.8 6.6 %collective-permute-done.6 = bf16[16,1024]{1,0:T(8,128)(2,1)S(1)} collective-permute-done((bf16[16,1024]{1,0:T(8,128)(2,1)S(1)}, bf16[16,1024]{1,0:T(8,128)(2,1)S(1)}, u32[]{:S(2)}, u32[]{:S(2)}) %collective-permute-start.6) | collective-permute-done | bytes 32800 | tf_op jit(solution)/shard_map/ppermute | solution.py:65
  56.2 0.9 fusion.8
  57.5 5.7 %psum.14 = f32[128]{0:T(128)S(1)} all-reduce(f32[128]{0:T(128)S(1)} %fusion.1), channel_id=1, replica_groups=mesh['tp'=8,'dp'=4] {'dp'}, use_global_device_ids=true, to_apply=%region_2.4 | all-reduce | flops 128 | bytes 1024 | tf_op jit(solution)/shard_map/psum | solution.py:75
  63.2 11.0 %reduce-scatter.5.cloned.1.call-done = f32[32,128]{1,0:T(8,128)} async-done(((f32[128,128]{1,0:T(8,128)}), f32[32,128]{1,0:T(8,128)}) %reduce-scatter.5.cloned.1.call-update) | async-done | bytes 16400 | tf_op jit(solution)/shard_map/reduce_scatter | solution.py:77
  77.2 5.2 %all_gather.6 = bf16[128,128]{1,0:T(8,128)(2,1)S(1)} all-gather(bf16[32,128]{1,0:T(8,128)(2,1)S(1)} %fusion.59), channel_id=1, replica_groups=mesh['tp'=8,'dp'=4] {'dp'}, dimensions={0}, use_global_device_ids=true | all-gather | bytes 40960 | tf_op jit(solution)/shard_map/all_gather | solution.py:95
  82.8 1.1 pad_maximum_fusion
  84.0 64.4 %reduce-scatter.7.cloned.1.call-done = f32[16,2048]{1,0:T(8,128)} async-done(((f32[128,2048]{1,0:T(8,128)}), f32[16,2048]{1,0:T(8,128)}) %reduce-scatter.7.cloned.1.call-update) | async-done | bytes 131088 | tf_op jit(solution)/shard_map/reduce_scatter | solution.py:98
  148.3 0.9 fusion.48
  149.2 1.1 collective-permute-start.7
  150.4 5.6 %collective-permute-done.7 = bf16[16,1024]{1,0:T(8,128)(2,1)S(1)} collective-permute-done((bf16[16,1024]{1,0:T(8,128)(2,1)S(1)}, bf16[16,1024]{1,0:T(8,128)(2,1)S(1)}, u32[]{:S(2)}, u32[]{:S(2)}) %collective-permute-start.7) | collective-permute-done | bytes 32800 | tf_op jit(solution)/shard_map/ppermute | solution.py:65
  155.9 6.6 %collective-permute-done.8 = bf16[16,1024]{1,0:T(8,128)(2,1)S(1)} collective-permute-done((bf16[16,1024]{1,0:T(8,128)(2,1)S(1)}, bf16[16,1024]{1,0:T(8,128)(2,1)S(1)}, u32[]{:S(2)}, u32[]{:S(2)}) %collective-permute-start.8) | collective-permute-done | bytes 32800 | tf_op jit(solution)/shard_map/ppermute | solution.py:65
  162.5 6.7 %collective-permute-done.9 = bf16[16,1024]{1,0:T(8,128)(2,1)S(1)} collective-permute-done((bf16[16,1024]{1,0:T(8,128)(2,1)S(1)}, bf16[16,1024]{1,0:T(8,128)(2,1)S(1)}, u32[]{:S(2)}, u32[]{:S(2)}) %collective-permute-start.9) | collective-permute-done | bytes 32800 | tf_op jit(solution)/shard_map/ppermute | solution.py:65
  169.2 6.6 %collective-permute-done.10 = bf16[16,1024]{1,0:T(8,128)(2,1)S(1)} collective-permute-done((bf16[16,1024]{1,0:T(8,128)(2,1)S(1)}, bf16[16,1024]{1,0:T(8,128)(2,1)S(1)}, u32[]{:S(2)}, u32[]{:S(2)}) %collective-permute-start.10) | collective-permute-done | bytes 32800 | tf_op jit(solution)/shard_map/ppermute | solution.py:65
  175.9 6.6 %collective-permute-done.11 = bf16[16,1024]{1,0:T(8,128)(2,1)S(1)} collective-permute-done((bf16[16,1024]{1,0:T(8,128)(2,1)S(1)}, bf16[16,1024]{1,0:T(8,128)(2,1)S(1)}, u32[]{:S(2)}, u32[]{:S(2)}) %collective-permute-start.11) | collective-permute-done | bytes 32800 | tf_op jit(solution)/shard_map/ppermute | solution.py:65
  182.5 6.6 %collective-permute-done.12 = bf16[16,1024]{1,0:T(8,128)(2,1)S(1)} collective-permute-done((bf16[16,1024]{1,0:T(8,128)(2,1)S(1)}, bf16[16,1024]{1,0:T(8,128)(2,1)S(1)}, u32[]{:S(2)}, u32[]{:S(2)}) %collective-permute-start.12) | collective-permute-done | bytes 32800 | tf_op jit(solution)/shard_map/ppermute | solution.py:65
  189.1 6.6 %collective-permute-done.13 = bf16[16,1024]{1,0:T(8,128)(2,1)S(1)} collective-permute-done((bf16[16,1024]{1,0:T(8,128)(2,1)S(1)}, bf16[16,1024]{1,0:T(8,128)(2,1)S(1)}, u32[]{:S(2)}, u32[]{:S(2)}) %collective-permute-start.13) | collective-permute-done | bytes 32800 | tf_op jit(solution)/shard_map/ppermute | solution.py:65
  195.8 0.9 fusion.6
  197.0 5.7 %psum.15 = f32[128]{0:T(128)S(1)} all-reduce(f32[128]{0:T(128)S(1)} %fusion.3), channel_id=1, replica_groups=mesh['tp'=8,'dp'=4] {'dp'}, use_global_device_ids=true, to_apply=%region_6.8 | all-reduce | flops 128 | bytes 1024 | tf_op jit(solution)/shard_map/psum | solution.py:75
  202.7 10.9 %reduce-scatter.9.cloned.1.call-done = f32[32,128]{1,0:T(8,128)} async-done(((f32[128,128]{1,0:T(8,128)}), f32[32,128]{1,0:T(8,128)}) %reduce-scatter.9.cloned.1.call-update) | async-done | bytes 16400 | tf_op jit(solution)/shard_map/reduce_scatter | solution.py:77
  216.3 5.2 %all_gather.7 = bf16[128,128]{1,0:T(8,128)(2,1)S(1)} all-gather(bf16[32,128]{1,0:T(8,128)(2,1)S(1)} %fusion.67), channel_id=1, replica_groups=mesh['tp'=8,'dp'=4] {'dp'}, dimensions={0}, use_global_device_ids=true | all-gather | bytes 40960 | tf_op jit(solution)/shard_map/all_gather | solution.py:95
  222.0 1.1 pad_maximum_fusion.1
  223.3 0.9 copy.27
  224.2 63.3 %reduce-scatter.11.cloned.1.call-done = f32[16,2048]{1,0:T(8,128)} async-done(((f32[128,2048]{1,0:T(8,128)}), f32[16,2048]{1,0:T(8,128)}) %reduce-scatter.11.cloned.1.call-update) | async-done | bytes 131088 | tf_op jit(solution)/shard_map/reduce_scatter | solution.py:98
  287.4 1.5 fusion.49
  (92 shorter events, 8.6 us)
Async XLA Ops:
  7.2 67.0 %reduce-scatter.5.cloned.1.call-start = ((), (), s32[]{:S(2)}) async-start(), calls=%async_computation.4 | async-start | bytes 81920 | tf_op jit(solution)/shard_map/reduce_scatter | solution.py:77
  7.2 8.2 %collective-permute-start = (bf16[16,1024]{1,0:T(8,128)(2,1)}, bf16[16,1024]{1,0:T(8,128)(2,1)S(1)}, u32[]{:S(2)}, u32[]{:S(2)}) collective-permute-start(bf16[16,1024]{1,0:T(8,128)(2,1)} %param.14), channel_id=1, source_target_pairs={{0,4},{4,8},{8,12},{12,16},{16,20},{20,24},{24,28},{28,0},{1,5},{5... | collective-permute-start | bytes 98312 | tf_op jit(solution)/shard_map/ppermute | solution.py:65
  15.4 6.6 %collective-permute-start.1 = (bf16[16,1024]{1,0:T(8,128)(2,1)S(1)}, bf16[16,1024]{1,0:T(8,128)(2,1)S(1)}, u32[]{:S(2)}, u32[]{:S(2)}) collective-permute-start(bf16[16,1024]{1,0:T(8,128)(2,1)S(1)} %collective-permute-done), channel_id=1, source_target_pairs={{0,4},{4,8},{8,12},{12,16},{16,20},{20,24},{24,28},{28,0},{1,5},{5... | collective-permute-start | bytes 98312 | tf_op jit(solution)/shard_map/ppermute | solution.py:65
  22.0 6.6 %collective-permute-start.2 = (bf16[16,1024]{1,0:T(8,128)(2,1)S(1)}, bf16[16,1024]{1,0:T(8,128)(2,1)S(1)}, u32[]{:S(2)}, u32[]{:S(2)}) collective-permute-start(bf16[16,1024]{1,0:T(8,128)(2,1)S(1)} %collective-permute-done.1), channel_id=1, source_target_pairs={{0,4},{4,8},{8,12},{12,16},{16,20},{20,24},{24,28},{28,0},{1,5},{5... | collective-permute-start | bytes 98312 | tf_op jit(solution)/shard_map/ppermute | solution.py:65
  22.0 6.6 %copy-start.10 = (f32[2,8]{1,0:T(2,128)S(1)}, f32[2,8]{1,0:T(2,128)}, u32[]{:S(2)}) copy-start(f32[2,8]{1,0:T(2,128)} %param.19) | copy-start | bytes 196
  22.0 13.2 %copy-start.7 = (f32[2,8,64]{2,1,0:T(8,128)S(1)}, f32[2,8,64]{2,1,0:T(8,128)}, u32[]{:S(2)}) copy-start(f32[2,8,64]{2,1,0:T(8,128)} %param.18) | copy-start | bytes 12292
  22.0 13.2 %copy-start.8 = (f32[2,8,64]{2,1,0:T(8,128)S(1)}, f32[2,8,64]{2,1,0:T(8,128)}, u32[]{:S(2)}) copy-start(f32[2,8,64]{2,1,0:T(8,128)} %param.17) | copy-start | bytes 12292
  22.0 34.2 %copy-start.12 = (bf16[2,1024,128]{2,1,0:T(8,128)(2,1)S(1)}, bf16[2,1024,128]{2,1,0:T(8,128)(2,1)}, u32[]{:S(2)}) copy-start(bf16[2,1024,128]{2,1,0:T(8,128)(2,1)} %param.16) | copy-start | bytes 1572868
  28.6 6.6 %collective-permute-start.3 = (bf16[16,1024]{1,0:T(8,128)(2,1)S(1)}, bf16[16,1024]{1,0:T(8,128)(2,1)S(1)}, u32[]{:S(2)}, u32[]{:S(2)}) collective-permute-start(bf16[16,1024]{1,0:T(8,128)(2,1)S(1)} %collective-permute-done.2), channel_id=1, source_target_pairs={{0,4},{4,8},{8,12},{12,16},{16,20},{20,24},{24,28},{28,0},{1,5},{5... | collective-permute-start | bytes 98312 | tf_op jit(solution)/shard_map/ppermute | solution.py:65
  35.2 7.0 %collective-permute-start.4 = (bf16[16,1024]{1,0:T(8,128)(2,1)S(1)}, bf16[16,1024]{1,0:T(8,128)(2,1)S(1)}, u32[]{:S(2)}, u32[]{:S(2)}) collective-permute-start(bf16[16,1024]{1,0:T(8,128)(2,1)S(1)} %collective-permute-done.3), channel_id=1, source_target_pairs={{0,4},{4,8},{8,12},{12,16},{16,20},{20,24},{24,28},{28,0},{1,5},{5... | collective-permute-start | bytes 98312 | tf_op jit(solution)/shard_map/ppermute | solution.py:65
  35.2 6.9 %copy-start.9 = (f32[2,1024]{1,0:T(2,128)S(1)}, f32[2,1024]{1,0:T(2,128)}, u32[]{:S(2)}) copy-start(f32[2,1024]{1,0:T(2,128)} %param.15) | copy-start | bytes 24580
  35.4 13.4 %copy-start.11 = (f32[2,128]{1,0:T(2,128)S(1)}, f32[2,128]{1,0:T(2,128)}, u32[]{:S(2)}) copy-start(f32[2,128]{1,0:T(2,128)} %param.22) | copy-start | bytes 3076
  42.2 6.6 %collective-permute-start.5 = (bf16[16,1024]{1,0:T(8,128)(2,1)S(1)}, bf16[16,1024]{1,0:T(8,128)(2,1)S(1)}, u32[]{:S(2)}, u32[]{:S(2)}) collective-permute-start(bf16[16,1024]{1,0:T(8,128)(2,1)S(1)} %collective-permute-done.4), channel_id=1, source_target_pairs={{0,4},{4,8},{8,12},{12,16},{16,20},{20,24},{24,28},{28,0},{1,5},{5... | collective-permute-start | bytes 98312 | tf_op jit(solution)/shard_map/ppermute | solution.py:65
  48.8 6.6 %collective-permute-start.6 = (bf16[16,1024]{1,0:T(8,128)(2,1)S(1)}, bf16[16,1024]{1,0:T(8,128)(2,1)S(1)}, u32[]{:S(2)}, u32[]{:S(2)}) collective-permute-start(bf16[16,1024]{1,0:T(8,128)(2,1)S(1)} %collective-permute-done.5), channel_id=1, source_target_pairs={{0,4},{4,8},{8,12},{12,16},{16,20},{20,24},{24,28},{28,0},{1,5},{5... | collective-permute-start | bytes 98312 | tf_op jit(solution)/shard_map/ppermute | solution.py:65
  55.5 0.8 copy-start.2
  57.2 17.9 %copy-start.3 = (f32[2,8,16,128]{3,2,1,0:T(8,128)S(1)}, f32[2,8,16,128]{3,2,1,0:T(8,128)}, u32[]{:S(2)}) copy-start(f32[2,8,16,128]{3,2,1,0:T(8,128)} %param.20) | copy-start | bytes 393220
  57.2 91.1 %reduce-scatter.7.cloned.1.call-start = ((), (), s32[]{:S(2)}) async-start(), calls=%async_computation.5 | async-start | bytes 1179648 | tf_op jit(solution)/shard_map/reduce_scatter | solution.py:98
  75.5 0.9 copy-start.4
  75.5 6.9 %copy-start = (bf16[2,128,1024]{2,1,0:T(8,128)(2,1)S(1)}, bf16[2,128,1024]{2,1,0:T(8,128)(2,1)}, u32[]{:S(2)}) copy-start(bf16[2,128,1024]{2,1,0:T(8,128)(2,1)} %param.24) | copy-start | bytes 1572868
  76.4 0.7 copy-start.6
  76.8 5.8 %copy-start.1 = (bf16[2,128,1024]{2,1,0:T(8,128)(2,1)S(1)}, bf16[2,128,1024]{2,1,0:T(8,128)(2,1)}, u32[]{:S(2)}) copy-start(bf16[2,128,1024]{2,1,0:T(8,128)(2,1)} %param.23) | copy-start | bytes 1572868
  83.9 129.7 %reduce-scatter.9.cloned.1.call-start = ((), (), s32[]{:S(2)}) async-start(), calls=%async_computation.6 | async-start | bytes 81920 | tf_op jit(solution)/shard_map/reduce_scatter | solution.py:77
  149.2 6.7 %collective-permute-start.7 = (bf16[16,1024]{1,0:T(8,128)(2,1)S(1)}, bf16[16,1024]{1,0:T(8,128)(2,1)S(1)}, u32[]{:S(2)}, u32[]{:S(2)}) collective-permute-start(bf16[16,1024]{1,0:T(8,128)(2,1)S(1)} %fusion.48), channel_id=1, source_target_pairs={{0,4},{4,8},{8,12},{12,16},{16,20},{20,24},{24,28},{28,0},{1,5},{5... | collective-permute-start | bytes 98312 | tf_op jit(solution)/shard_map/ppermute | solution.py:65
  155.9 6.6 %collective-permute-start.8 = (bf16[16,1024]{1,0:T(8,128)(2,1)S(1)}, bf16[16,1024]{1,0:T(8,128)(2,1)S(1)}, u32[]{:S(2)}, u32[]{:S(2)}) collective-permute-start(bf16[16,1024]{1,0:T(8,128)(2,1)S(1)} %collective-permute-done.7), channel_id=1, source_target_pairs={{0,4},{4,8},{8,12},{12,16},{16,20},{20,24},{24,28},{28,0},{1,5},{5... | collective-permute-start | bytes 98312 | tf_op jit(solution)/shard_map/ppermute | solution.py:65
  162.5 6.7 %collective-permute-start.9 = (bf16[16,1024]{1,0:T(8,128)(2,1)S(1)}, bf16[16,1024]{1,0:T(8,128)(2,1)S(1)}, u32[]{:S(2)}, u32[]{:S(2)}) collective-permute-start(bf16[16,1024]{1,0:T(8,128)(2,1)S(1)} %collective-permute-done.8), channel_id=1, source_target_pairs={{0,4},{4,8},{8,12},{12,16},{16,20},{20,24},{24,28},{28,0},{1,5},{5... | collective-permute-start | bytes 98312 | tf_op jit(solution)/shard_map/ppermute | solution.py:65
  169.2 6.6 %collective-permute-start.10 = (bf16[16,1024]{1,0:T(8,128)(2,1)S(1)}, bf16[16,1024]{1,0:T(8,128)(2,1)S(1)}, u32[]{:S(2)}, u32[]{:S(2)}) collective-permute-start(bf16[16,1024]{1,0:T(8,128)(2,1)S(1)} %collective-permute-done.9), channel_id=1, source_target_pairs={{0,4},{4,8},{8,12},{12,16},{16,20},{20,24},{24,28},{28,0},{1,5},{5... | collective-permute-start | bytes 98312 | tf_op jit(solution)/shard_map/ppermute | solution.py:65
  175.9 6.6 %collective-permute-start.11 = (bf16[16,1024]{1,0:T(8,128)(2,1)S(1)}, bf16[16,1024]{1,0:T(8,128)(2,1)S(1)}, u32[]{:S(2)}, u32[]{:S(2)}) collective-permute-start(bf16[16,1024]{1,0:T(8,128)(2,1)S(1)} %collective-permute-done.10), channel_id=1, source_target_pairs={{0,4},{4,8},{8,12},{12,16},{16,20},{20,24},{24,28},{28,0},{1,5},{5... | collective-permute-start | bytes 98312 | tf_op jit(solution)/shard_map/ppermute | solution.py:65
  182.5 6.6 %collective-permute-start.12 = (bf16[16,1024]{1,0:T(8,128)(2,1)S(1)}, bf16[16,1024]{1,0:T(8,128)(2,1)S(1)}, u32[]{:S(2)}, u32[]{:S(2)}) collective-permute-start(bf16[16,1024]{1,0:T(8,128)(2,1)S(1)} %collective-permute-done.11), channel_id=1, source_target_pairs={{0,4},{4,8},{8,12},{12,16},{16,20},{20,24},{24,28},{28,0},{1,5},{5... | collective-permute-start | bytes 98312 | tf_op jit(solution)/shard_map/ppermute | solution.py:65
  189.1 6.6 %collective-permute-start.13 = (bf16[16,1024]{1,0:T(8,128)(2,1)S(1)}, bf16[16,1024]{1,0:T(8,128)(2,1)S(1)}, u32[]{:S(2)}, u32[]{:S(2)}) collective-permute-start(bf16[16,1024]{1,0:T(8,128)(2,1)S(1)} %collective-permute-done.12), channel_id=1, source_target_pairs={{0,4},{4,8},{8,12},{12,16},{16,20},{20,24},{24,28},{28,0},{1,5},{5... | collective-permute-start | bytes 98312 | tf_op jit(solution)/shard_map/ppermute | solution.py:65
  196.7 90.7 %reduce-scatter.11.cloned.1.call-start = ((), (), s32[]{:S(2)}) async-start(), calls=%async_computation.7 | async-start | bytes 1179648 | tf_op jit(solution)/shard_map/reduce_scatter | solution.py:98
  215.5 0.7 copy-start.5
Sparse Core Ops, SparseCore 0:
  57.3 16.8 reduce-scatter.4
  84.1 64.2 reduce-scatter.6
  196.8 16.7 reduce-scatter.8
  223.2 64.2 reduce-scatter.10
